TPU v7x, 32 devices: a whole 2x2x4 slice. The times are simulated.
32 devices in a mesh: sp: 8 (over z, y), tp: 4 (over x, core).
Axes of the slice: x: 2, y: 2, z: 4, core: 2. Of those that a mesh axis runs over, the one named last changes fastest.
Arguments:
- tokens: bfloat16 [4096, 2048], P('sp', 'tp'), may hold values from -400 to 400
- norm_gain: float32 [2048], replicated, may hold values from 0.1 to 1.9
- query_weight: bfloat16 [2048, 1024], P(None, 'tp'), may hold values from -0.37306796 to 0.37306796
- key_weight: bfloat16 [2048, 1024], P(None, 'tp'), may hold values from -0.2625825 to 0.2625825
- value_weight: bfloat16 [2048, 1024], P(None, 'tp'), may hold values from -0.125 to 0.125
- outer_gate_weight: bfloat16 [2048, 1024], P(None, 'tp'), may hold values from -0.125 to 0.125
- inner_gate_weight: bfloat16 [2048, 1024], P(None, 'tp'), may hold values from -0.125 to 0.125
- conv_input_weight: bfloat16 [2048, 1024], P(None, 'tp'), may hold values from -0.125 to 0.125
- conv_taps: float32 [3, 1024], P(None, 'tp'), may hold values from -3.5 to 3.5
- lambdas: float32 [8], P('tp'), may hold values from 0.3 to 0.8
- head_gain: float32 [128], replicated, may hold values from 0.1 to 1.9
- attn_out_weight: bfloat16 [1024, 2048], P(None, 'tp'), may hold values from -0.125 to 0.125
- conv_out_weight: bfloat16 [1024, 2048], P(None, 'tp'), may hold values from -0.125 to 0.125
Outputs:
- mixed_out: bfloat16 [4096, 2048], P('sp', 'tp')
- log_totals: float32 [8, 2, 4096], P('tp', None, 'sp')
All inputs are finite; a program needn't handle non-finite values.
Results may differ from a plain program's by a relative error of at most 0.014.
The roundings to bfloat16 on the way count: a program that leaves them out, or rounds other values in their place, can miss the bound.
Values may be sent and summed in bfloat16 or wider, within the bound.
No kernel may reach another device: no remote copies, remote signals or barrier semaphores. Data moves between devices by JAX's collectives and lax.ppermute only.
A program may use at most 128 MiB of HBM per device.

v0:
```python
import math

import jax
import jax.numpy as jnp
from jax import lax
from jax.sharding import PartitionSpec as P

NORM_EPS = 1e-06
HEAD_EPS = 1e-05
ROPE_BASE = 500000.0
MASKED = -1e30
HEAD_SCALE = 0.8


def shifted(block, axis, distance):
    devices = range(lax.axis_size(axis))
    route = [(i - distance, i) for i in devices if i - distance in devices]
    return lax.ppermute(block, axis, route)


def rotate(field_in, positions):
    half_dim = field_in.shape[-1] // 2
    frequency = ROPE_BASE ** (-jnp.arange(half_dim, dtype=jnp.float32) * 2.0 / field_in.shape[-1])
    angles = positions[:, None] * frequency[None, :]
    cosine = jnp.cos(angles)[:, None, None, :]
    sine_part = jnp.sin(angles)[:, None, None, :]
    first_half = field_in[..., :half_dim]
    second_half = field_in[..., half_dim:]
    return jnp.concatenate(
        [
            first_half * cosine - second_half * sine_part,
            second_half * cosine + first_half * sine_part,
        ],
        axis=-1,
    )


def add_products(block_in, norm_gain, weights):
    floats = block_in.astype(jnp.float32)
    scaled = (floats * norm_gain[None, :]).astype(jnp.bfloat16)
    products = tuple(
        (jnp.dot(scaled, weight, preferred_element_type=jnp.float32) for weight in weights)
    )
    return (jnp.sum(floats * floats, axis=1, keepdims=True),) + products


def over_shards(step_fn, running, arrays, anchor, local_rows):
    shard_count = arrays[0].shape[0] // local_rows
    group_size = math.gcd(shard_count, max(1, 2048 // local_rows))
    block_rows = group_size * local_rows
    steps_count = shard_count // group_size
    stacked = tuple(
        (member.reshape((steps_count, block_rows) + member.shape[1:]) for member in arrays)
    )

    def scan_step(carried, scan_items):
        members, step_index = scan_items
        return (step_fn(carried, members, anchor + step_index * block_rows), None)

    result, unused = lax.scan(
        scan_step, running, (stacked, jnp.arange(steps_count, dtype=jnp.int32))
    )
    return result


def per_device(
    tokens,
    norm_gain,
    query_weight,
    key_weight,
    value_weight,
    outer_gate_weight,
    inner_gate_weight,
    conv_input_weight,
    conv_taps,
    lambdas,
    head_gain,
    attn_out_weight,
    conv_out_weight,
):
    local_rows = tokens.shape[0]
    local_heads = lambdas.shape[0]
    head_dim = query_weight.shape[1] // (2 * local_heads)
    value_dim = 2 * head_dim
    taps_count = conv_taps.shape[0]
    width_all = norm_gain.shape[0]
    columns_dev = query_weight.shape[1]
    attn_weights = (query_weight, key_weight, value_weight)
    conv_weights = (outer_gate_weight, inner_gate_weight, conv_input_weight)
    squares, query_raw, key_raw, value_raw, outer_raw, inner_raw, signal_raw = add_products(
        lax.all_gather(tokens, "tp", axis=1, tiled=True), norm_gain, attn_weights + conv_weights
    )
    inverse_rms = lax.rsqrt(squares / width_all + NORM_EPS)
    query_pos = lax.axis_index("sp") * local_rows + jnp.arange(local_rows, dtype=jnp.int32)
    positions = query_pos.astype(jnp.float32)
    queries = rotate(
        (inverse_rms * query_raw).reshape(local_rows, local_heads, 2, head_dim), positions
    ).astype(jnp.bfloat16)
    key_rows = rotate(
        (inverse_rms * key_raw).reshape(local_rows, local_heads, 2, head_dim), positions
    ).astype(jnp.bfloat16)
    values = (
        (inverse_rms * value_raw).astype(jnp.bfloat16).reshape(local_rows, local_heads, value_dim)
    )
    outer_gate = (inverse_rms * outer_raw).astype(jnp.bfloat16)
    inner_gate = (inverse_rms * inner_raw).astype(jnp.bfloat16)
    signal = (inverse_rms * signal_raw).astype(jnp.bfloat16)
    conv_in = (inner_gate.astype(jnp.float32) * signal.astype(jnp.float32)).astype(jnp.bfloat16)
    rim_rows = shifted(conv_in[local_rows - (taps_count - 1) :], "sp", 1)
    padded = jnp.concatenate([rim_rows, conv_in], axis=0)
    summed = jnp.zeros((local_rows, columns_dev), jnp.float32)
    for tap_index in range(taps_count):
        summed = summed + conv_taps[tap_index][None, :] * padded[
            tap_index : tap_index + local_rows
        ].astype(jnp.float32)
    conv_out = (outer_gate.astype(jnp.float32) * summed).astype(jnp.bfloat16)
    scale_factor = head_dim ** (-0.5)

    def block_scores(key_block, key_anchor):
        scores = (
            jnp.einsum("qhcd,khcd->hcqk", queries, key_block, preferred_element_type=jnp.float32)
            * scale_factor
        )
        visible = (
            query_pos[:, None]
            >= (key_anchor + jnp.arange(key_block.shape[0], dtype=jnp.int32))[None, :]
        )
        return (jnp.where(visible, scores, MASKED), visible)

    def stats_step(running, members, key_anchor):
        max_before, sum_before = running
        scores, visible = block_scores(members[0], key_anchor)
        max_after = jnp.maximum(max_before, jnp.max(scores, axis=-1))
        exponent = jnp.where(visible, jnp.exp(scores - max_after[..., None]), 0.0)
        return (
            max_after,
            sum_before * jnp.exp(max_before - max_after) + jnp.sum(exponent, axis=-1),
        )

    stats_init = (
        jnp.full((local_heads, 2, local_rows), MASKED, jnp.float32),
        jnp.zeros((local_heads, 2, local_rows), jnp.float32),
    )
    value_init = jnp.zeros((local_rows, local_heads, value_dim), jnp.float32)

    def value_step_with(row_max, row_sum):

        def value_step(running, members, key_anchor):
            scores, visible = block_scores(members[0], key_anchor)
            normalized = jnp.where(
                visible, jnp.exp(scores - row_max[..., None]) / row_sum[..., None], 0.0
            )
            weights = (normalized[:, 0] - lambdas[:, None, None] * normalized[:, 1]).astype(
                jnp.bfloat16
            )
            return running + jnp.einsum(
                "hqk,khv->qhv", weights, members[1], preferred_element_type=jnp.float32
            )

        return value_step

    all_keys, all_values = (
        lax.all_gather(key_rows, "sp", axis=0, tiled=True),
        lax.all_gather(values, "sp", axis=0, tiled=True),
    )
    row_max, row_sum = over_shards(stats_step, stats_init, (all_keys,), 0, local_rows)
    head_mix = over_shards(
        value_step_with(row_max, row_sum), value_init, (all_keys, all_values), 0, local_rows
    )
    log_totals = row_max + jnp.log(row_sum)
    normed = (
        head_mix
        * lax.rsqrt(jnp.mean(head_mix * head_mix, axis=-1, keepdims=True) + HEAD_EPS)
        * head_gain[None, None, :]
        * HEAD_SCALE
    )
    attn_out = normed.astype(jnp.bfloat16).reshape(local_rows, local_heads * value_dim)
    running = jnp.zeros((local_rows, attn_out_weight.shape[1]), jnp.float32)
    running = jnp.dot(
        lax.all_gather(attn_out, "tp", axis=1, tiled=True),
        attn_out_weight,
        preferred_element_type=jnp.float32,
    )
    mixed_out = running + jnp.dot(
        lax.all_gather(conv_out, "tp", axis=1, tiled=True),
        conv_out_weight,
        preferred_element_type=jnp.float32,
    )
    return (mixed_out.astype(jnp.bfloat16), log_totals)


def solution(mesh):
    in_specs = (
        P("sp", "tp"),
        P(),
        P(None, "tp"),
        P(None, "tp"),
        P(None, "tp"),
        P(None, "tp"),
        P(None, "tp"),
        P(None, "tp"),
        P(None, "tp"),
        P("tp"),
        P(),
        P(None, "tp"),
        P(None, "tp"),
    )
    out_specs = (P("sp", "tp"), P("tp", None, "sp"))
    return jax.shard_map(
        per_device, mesh=mesh, in_specs=in_specs, out_specs=out_specs, check_vma=False
    )
```

profile of v0, /device:TPU:0, one launch (start us, length us, event | category | flops | bytes accessed | tf_op | source)
XLA Modules:
  0.0 211.2 jit_solution(9740739602610465239)
XLA Ops:
  8.3 26.6 %all-gather.6.cloned.1.call-done = bf16[512,2048]{1,0:T(8,128)(2,1)} async-done(((bf16[512,512]{1,0:T(8,128)(2,1)}), bf16[512,2048]{1,0:T(8,128)(2,1)}) %all-gather.6.cloned.1.call-update) | async-done | bytes 2097168 | tf_op jit(solution)/shard_map/all_gather | solution.py:91
  34.9 2.2 %fusion.32 = f32[512]{0:T(512)S(1)} fusion(bf16[512,2048]{1,0:T(8,128)(2,1)} %all-gather.6.cloned.1.call-done), kind=kLoop, calls=%fused_computation.40 | loop fusion | flops 3145216 | bytes 2099200 | tf_op jit(solution)/shard_map/reduce_sum | solution.py:44
  37.1 2.6 %convolution_multiply_fusion.4 = f32[512,256]{0,1:T(8,128)S(1)} fusion(bf16[2048,256]{1,0:T(8,128)(2,1)} %param.20, bf16[512,2048]{1,0:T(8,128)(2,1)} %all-gather.6.cloned.1.call-done, f32[2048]{0:T(1024)} %param.18, f32[512]{0:T(512)S(1)} %add_rsqrt_fusion.1), kind=kOutput, calls=%fused_computation.49 | convolution fusion | flops 540147712 | bytes 3680256 | tf_op jit(solution)/shard_map/dot_general | solution.py:42
  41.6 2.7 %fusion.35 = bf16[512,256]{0,1:T(8,128)(2,1)} fusion(bf16[2048,256]{1,0:T(8,128)(2,1)} %param.21, bf16[512,2048]{1,0:T(8,128)(2,1)S(1)} %copy-done.1, f32[2048]{0:T(1024)} %param.18, f32[512]{0:T(512)S(1)} %add_rsqrt_fusion.1), kind=kOutput, calls=%fused_computation.51 | convolution fusion | flops 540278784 | bytes 3418112 | tf_op jit(solution)/shard_map/dot_general | solution.py:42
  44.3 1.8 copy.21
  46.9 45.2 %all-gather.10.cloned.1.call-done = bf16[4096,2,2,64]{0,3,2,1:T(8,128)(2,1)} async-done(((bf16[512,2,2,64]{0,3,2,1:T(8,128)(2,1)}), bf16[4096,2,2,64]{0,3,2,1:T(8,128)(2,1)}) %all-gather.10.cloned.1.call-update) | async-done | bytes 2097168 | tf_op jit(solution)/shard_map/all_gather | solution.py:163
  92.1 1.7 copy.34
  93.8 18.6 %while.24 = (s32[]{:T(128)}, f32[2,2,512]{2,1,0:T(2,128)S(1)}, f32[2,2,512]{2,1,0:T(2,128)S(1)}, s32[2]{0:T(128)S(1)}, bf16[2,2048,2,2,64]{1,4,3,2,0:T(8,128)(2,...) while((s32[]{:T(128)}, f32[2,2,512]{2,1,0:T(2,128)S(1)}, ...), condition=%wide.region_4.5_spmd.clone, body=%wide.region_1.4_spmd.clone.sunk | while | flops 571486720 | bytes 38138008 | solution.py:60
  95.9 3.0 %fusion.78 = (f32[2,2,512]{2,1,0:T(2,128)S(1)}, f32[2,2,2048,512]{3,2,1,0:T(8,128)S(1)}) fusion(pred[512,2048]{0,1:T(8,128)(4,1)S(1)} %broadcast_compare_fusion.4, bf16[512,2,2,64]{0,3,2,1:T(8,128)(2,1)S(1)} %get-tuple-element.355, bf16[2,2048,2,2,64]{1,4,3,2,0:T(8,128)(2,1)S(1)} %get-tuple-element.354, s32[]{:T(128)S(6)} %copy.38), kind=kOutput, calls=%fused_computation.4.clone.1 | convolution fusion | flops 549451776 | bytes 19144708 | tf_op jit(solution)/shard_map/while/body/eval_jaxpr/qhcd,khcd->hcqk/dot_general | solution.py:121
  98.9 4.2 %select_reduce_fusion.2 = f32[2,2,512]{2,1,0:T(2,128)S(1)} fusion(f32[2,2,2048,512]{3,2,1,0:T(8,128)S(1)} %get-tuple-element.319, f32[2,2,512]{2,1,0:T(2,128)S(1)} %fusion.79, pred[512,2048]{0,1:T(8,128)(4,1)S(1)} %broadcast_compare_fusion.4), kind=kLoop, calls=%fused_computation.3.clone.1 | loop fusion | flops 20969472 | bytes 17842176 | tf_op jit(solution)/shard_map/while/body/eval_jaxpr/reduce_sum | solution.py:137
  105.2 3.0 %fusion.78 = (f32[2,2,512]{2,1,0:T(2,128)S(1)}, f32[2,2,2048,512]{3,2,1,0:T(8,128)S(1)}) fusion(pred[512,2048]{0,1:T(8,128)(4,1)S(1)} %broadcast_compare_fusion.4, bf16[512,2,2,64]{0,3,2,1:T(8,128)(2,1)S(1)} %get-tuple-element.355, bf16[2,2048,2,2,64]{1,4,3,2,0:T(8,128)(2,1)S(1)} %get-tuple-element.354, s32[]{:T(128)S(6)} %copy.38), kind=kOutput, calls=%fused_computation.4.clone.1 | convolution fusion | flops 549451776 | bytes 19144708 | tf_op jit(solution)/shard_map/while/body/eval_jaxpr/qhcd,khcd->hcqk/dot_general | solution.py:121
  108.2 4.2 %select_reduce_fusion.2 = f32[2,2,512]{2,1,0:T(2,128)S(1)} fusion(f32[2,2,2048,512]{3,2,1,0:T(8,128)S(1)} %get-tuple-element.319, f32[2,2,512]{2,1,0:T(2,128)S(1)} %fusion.79, pred[512,2048]{0,1:T(8,128)(4,1)S(1)} %broadcast_compare_fusion.4), kind=kLoop, calls=%fused_computation.3.clone.1 | loop fusion | flops 20969472 | bytes 17842176 | tf_op jit(solution)/shard_map/while/body/eval_jaxpr/reduce_sum | solution.py:137
  112.5 29.0 %all-gather.8.cloned.1.call-done = bf16[4096,2,128]{2,0,1:T(8,128)(2,1)} async-done(((bf16[512,2,128]{2,0,1:T(8,128)(2,1)}), bf16[4096,2,128]{2,0,1:T(8,128)(2,1)}) %all-gather.8.cloned.1.call-update) | async-done | bytes 2097168 | tf_op jit(solution)/shard_map/all_gather | solution.py:164
  141.6 23.3 %while.25 = (s32[]{:T(128)}, f32[512,2,128]{0,2,1:T(8,128)}, bf16[2,2048,2,128]{3,1,0,2:T(8,128)(2,1)}, s32[2]{0:T(128)S(1)}, bf16[2,2048,2,2,64]{1,4,3,2,0:T(8,...) while((s32[]{:T(128)}, f32[512,2,128]{0,2,1:T(8,128)}, ...), condition=%wide.region_6.7_spmd.clone, body=%wide.region_5.6_spmd.clone.sunk | while | flops 1102318080 | bytes 51680008 | solution.py:60
  143.7 7.4 %fusion.85 = f32[2,2,512,2048]{2,3,1,0:T(8,128)S(1)} fusion(f32[2,2,512]{2,1,0:T(2,128)S(1)} %get-tuple-element.393, f32[2,2,512]{2,1,0:T(2,128)S(1)} %get-tuple-element.392, pred[512,2048]{0,1:T(8,128)(4,1)S(1)} %broadcast_compare_fusion.5, bf16[512,2,2,64]{0,3,2,1:T(8,128)(2,1)S(1)} %get-tuple-element.391, ...), kind=kOutput, calls=%fused_computation.20.clone.1 | convolution fusion | flops 557842432 | bytes 19152900 | tf_op jit(solution)/shard_map/while/body/eval_jaxpr/qhcd,khcd->hcqk/dot_general | solution.py:121
  155.3 7.4 %fusion.85 = f32[2,2,512,2048]{2,3,1,0:T(8,128)S(1)} fusion(f32[2,2,512]{2,1,0:T(2,128)S(1)} %get-tuple-element.393, f32[2,2,512]{2,1,0:T(2,128)S(1)} %get-tuple-element.392, pred[512,2048]{0,1:T(8,128)(4,1)S(1)} %broadcast_compare_fusion.5, bf16[512,2,2,64]{0,3,2,1:T(8,128)(2,1)S(1)} %get-tuple-element.391, ...), kind=kOutput, calls=%fused_computation.20.clone.1 | convolution fusion | flops 557842432 | bytes 19152900 | tf_op jit(solution)/shard_map/while/body/eval_jaxpr/qhcd,khcd->hcqk/dot_general | solution.py:121
  166.0 1.9 multiply_convert_fusion
  168.2 2.1 %fusion.42 = f32[512,256]{0,1:T(8,128)S(1)} fusion(bf16[2048,256]{1,0:T(8,128)(2,1)} %param.23, bf16[512,2048]{1,0:T(8,128)(2,1)S(1)} %copy-done.2, f32[2048]{0:T(1024)S(1)} %copy-done.17, f32[512]{0:T(512)S(1)} %copy-done.9), kind=kOutput, calls=%fused_computation.58 | convolution fusion | flops 540409856 | bytes 3680256 | tf_op jit(solution)/shard_map/dot_general | solution.py:42
  171.2 2.5 %collective-permute-start = (bf16[2,256]{0,1:T(8,128)(2,1)S(1)}, bf16[2,256]{0,1:T(8,128)(2,1)S(1)}, u32[]{:S(2)}, u32[]{:S(2)}) collective-permute-start(bf16[2,256]{0,1:T(8,128)(2,1)S(1)} %slice.54), channel_id=1, source_target_pairs={{0,4},{4,8},{8,12},{12,16},{16,20},{20,24},{24,28},{1,5},{5,9},{9,... | collective-permute-start | bytes 3080 | tf_op jit(solution)/shard_map/ppermute | solution.py:18
  173.7 1.9 collective-permute-done
  177.8 5.5 %all-gather.12.cloned.1.call-done = bf16[512,1024]{0,1:T(8,128)(2,1)} async-done(((bf16[512,256]{0,1:T(8,128)(2,1)}), bf16[512,1024]{0,1:T(8,128)(2,1)}) %all-gather.12.cloned.1.call-update) | async-done | bytes 1048592 | tf_op jit(solution)/shard_map/all_gather | solution.py:180
  183.3 2.0 fusion.54
  185.2 16.8 %all-gather.14.cloned.1.call-done = bf16[512,1024]{0,1:T(8,128)(2,1)} async-done(((bf16[512,256]{0,1:T(8,128)(2,1)}), bf16[512,1024]{0,1:T(8,128)(2,1)}) %all-gather.14.cloned.1.call-update) | async-done | bytes 1048592 | tf_op jit(solution)/shard_map/all_gather | solution.py:185
  202.0 2.8 %fusion.34 = bf16[512,512]{1,0:T(8,128)(2,1)} fusion(f32[512,512]{1,0:T(8,128)S(1)} %fusion.54, bf16[512,1024]{0,1:T(8,128)(2,1)} %all-gather.14.cloned.1.call-done, bf16[1024,512]{1,0:T(8,128)(2,1)S(1)} %copy-done.15), kind=kOutput, calls=%fused_computation.44 | convolution fusion | flops 537395200 | bytes 3670016 | tf_op jit(solution)/shard_map/dot_general | solution.py:184
  (98 shorter events, 18.1 us)
Async XLA Ops:
  7.2 176.1 %copy-start = (bf16[1024,512]{1,0:T(8,128)(2,1)S(1)}, bf16[1024,512]{1,0:T(8,128)(2,1)}, u32[]{:S(2)}) copy-start(bf16[1024,512]{1,0:T(8,128)(2,1)} %param.28) | copy-start | bytes 3145732
  7.2 32.6 %copy-start.16 = (f32[2048]{0:T(1024)S(1)}, f32[2048]{0:T(1024)}, u32[]{:S(2)}) copy-start(f32[2048]{0:T(1024)} %param.18) | copy-start | bytes 24580
  7.2 27.7 %all-gather.6.cloned.1.call-start = ((), (), s32[]{:S(2)}) async-start(), calls=%async_computation | async-start | bytes 2621440 | tf_op jit(solution)/shard_map/all_gather | solution.py:91
  7.9 84.1 %all-gather.10.cloned.1.call-start = ((), (), s32[]{:S(2)}) async-start(), calls=%async_computation.2 | async-start | bytes 2359296 | tf_op jit(solution)/shard_map/all_gather | solution.py:163
  34.9 4.9 %copy-start.1 = (bf16[512,2048]{1,0:T(8,128)(2,1)S(1)}, bf16[512,2048]{1,0:T(8,128)(2,1)}, u32[]{:S(2)}) copy-start(bf16[512,2048]{1,0:T(8,128)(2,1)} %all-gather.6.cloned.1.call-done) | copy-start | bytes 6291460
  34.9 4.9 %copy-start.12 = (bf16[2048,256]{1,0:T(8,128)(2,1)S(1)}, bf16[2048,256]{1,0:T(8,128)(2,1)}, u32[]{:S(2)}) copy-start(bf16[2048,256]{1,0:T(8,128)(2,1)} %param.19) | copy-start | bytes 3145732
  41.5 100.0 %all-gather.8.cloned.1.call-start = ((), (), s32[]{:S(2)}) async-start(), calls=%async_computation.1 | async-start | bytes 2359296 | tf_op jit(solution)/shard_map/all_gather | solution.py:164
  46.1 137.1 %all-gather.12.cloned.1.call-start = ((), (), s32[]{:S(2)}) async-start(), calls=%async_computation.3 | async-start | bytes 1310720 | tf_op jit(solution)/shard_map/all_gather | solution.py:180
  46.9 46.9 %copy-start.6 = (bf16[512,2,2,64]{0,3,2,1:T(8,128)(2,1)S(1)}, bf16[512,2,2,64]{0,3,2,1:T(8,128)(2,1)}, u32[]{:S(2)}) copy-start(bf16[512,2,2,64]{0,3,2,1:T(8,128)(2,1)} %pad_maximum_fusion.2) | copy-start | bytes 786436
  93.8 47.7 %copy-start.18 = (f32[2]{0:T(128)S(1)}, f32[2]{0:T(128)}, u32[]{:S(2)}) copy-start(f32[2]{0:T(128)} %param.26) | copy-start | bytes 28
  112.5 29.1 %copy-start.3 = (bf16[2,2048,2,2,64]{1,4,3,2,0:T(8,128)(2,1)}, bf16[2,2048,2,2,64]{1,4,3,2,0:T(8,128)(2,1)S(1)}, u32[]{:S(2)}) copy-start(bf16[2,2048,2,2,64]{1,4,3,2,0:T(8,128)(2,1)S(1)} %get-tuple-element.405) | copy-start | bytes 6291460
  141.5 24.4 %copy-start.10 = (f32[128]{0:T(128)S(1)}, f32[128]{0:T(128)}, u32[]{:S(2)}) copy-start(f32[128]{0:T(128)} %param.27) | copy-start | bytes 1540
  141.5 26.6 %copy-start.2 = (bf16[512,2048]{1,0:T(8,128)(2,1)S(1)}, bf16[512,2048]{1,0:T(8,128)(2,1)}, u32[]{:S(2)}) copy-start(bf16[512,2048]{1,0:T(8,128)(2,1)} %all-gather.6.cloned.1.call-done) | copy-start | bytes 6291460
  141.6 26.6 %copy-start.9 = (f32[512]{0:T(512)S(1)}, f32[512]{0:T(512)}, u32[]{:S(2)}) copy-start(f32[512]{0:T(512)} %copy-done.8) | copy-start | bytes 6148
  141.6 26.6 %copy-start.17 = (f32[2048]{0:T(1024)S(1)}, f32[2048]{0:T(1024)}, u32[]{:S(2)}) copy-start(f32[2048]{0:T(1024)} %param.18) | copy-start | bytes 24580
  143.6 7.5 %copy-start.4 = (f32[512,2,128]{0,2,1:T(8,128)S(1)}, f32[512,2,128]{0,2,1:T(8,128)}, u32[]{:S(2)}) copy-start(f32[512,2,128]{0,2,1:T(8,128)} %get-tuple-element.374) | copy-start | bytes 1572868 | tf_op jit(solution)/shard_map/while
  143.7 7.5 %copy-start.11 = (bf16[2,2048,2,128]{3,1,0,2:T(8,128)(2,1)S(1)}, bf16[2,2048,2,128]{3,1,0,2:T(8,128)(2,1)}, u32[]{:S(2)}) copy-start(bf16[2,2048,2,128]{3,1,0,2:T(8,128)(2,1)} %get-tuple-element.388) | copy-start | bytes 6291460 | tf_op jit(solution)/shard_map/while
  155.3 7.4 %copy-start.4 = (f32[512,2,128]{0,2,1:T(8,128)S(1)}, f32[512,2,128]{0,2,1:T(8,128)}, u32[]{:S(2)}) copy-start(f32[512,2,128]{0,2,1:T(8,128)} %get-tuple-element.374) | copy-start | bytes 1572868 | tf_op jit(solution)/shard_map/while
  155.3 7.4 %copy-start.11 = (bf16[2,2048,2,128]{3,1,0,2:T(8,128)(2,1)S(1)}, bf16[2,2048,2,128]{3,1,0,2:T(8,128)(2,1)}, u32[]{:S(2)}) copy-start(bf16[2,2048,2,128]{3,1,0,2:T(8,128)(2,1)} %get-tuple-element.388) | copy-start | bytes 6291460 | tf_op jit(solution)/shard_map/while
  167.9 5.8 %copy-start.7 = (f32[3,256]{1,0:T(4,128)S(1)}, f32[3,256]{1,0:T(4,128)}, u32[]{:S(2)}) copy-start(f32[3,256]{1,0:T(4,128)} %param.25) | copy-start | bytes 9220
  167.9 34.1 %all-gather.14.cloned.1.call-start = ((), (), s32[]{:S(2)}) async-start(), calls=%async_computation.4 | async-start | bytes 1310720 | tf_op jit(solution)/shard_map/all_gather | solution.py:185
  168.2 7.4 %copy-start.14 = (bf16[2048,256]{1,0:T(8,128)(2,1)S(1)}, bf16[2048,256]{1,0:T(8,128)(2,1)}, u32[]{:S(2)}) copy-start(bf16[2048,256]{1,0:T(8,128)(2,1)} %param.22) | copy-start | bytes 3145732
  171.2 4.3 %collective-permute-start = (bf16[2,256]{0,1:T(8,128)(2,1)S(1)}, bf16[2,256]{0,1:T(8,128)(2,1)S(1)}, u32[]{:S(2)}, u32[]{:S(2)}) collective-permute-start(bf16[2,256]{0,1:T(8,128)(2,1)S(1)} %slice.54), channel_id=1, source_target_pairs={{0,4},{4,8},{8,12},{12,16},{16,20},{20,24},{24,28},{1,5},{5,9},{9,... | collective-permute-start | bytes 3080 | tf_op jit(solution)/shard_map/ppermute | solution.py:18
  177.2 24.8 %copy-start.15 = (bf16[1024,512]{1,0:T(8,128)(2,1)S(1)}, bf16[1024,512]{1,0:T(8,128)(2,1)}, u32[]{:S(2)}) copy-start(bf16[1024,512]{1,0:T(8,128)(2,1)} %param.29) | copy-start | bytes 3145732
  (4 other events, 8.2 us)
Sparse Core Ops, SparseCore 0:
  9.6 25.2 all-gather.5
  41.6 50.3 all-gather.9
  94.2 47.2 all-gather.7
  168.0 15.2 all-gather.11
  185.2 16.6 all-gather.13
where the time goes:
time: 212 us; the launch traced here: 211 us
  waiting for transfers between devices  126 us (59%)
  matrix products  38.8 us (18%)
  other arithmetic  19.3 us (9%)
  between operations  14.1 us (7%)
  local copies, waits for them, and re-layouts  7.83 us (4%)
  starting transfers between devices  2.84 us (1%)
  loops' own time  2.83 us (1%)
    all_gather x1, waiting for transfers between devices, per_device(): lax.all_gather(key_rows, 'sp', axis=0, tiled=True)  45.2 us
    all_gather x1, waiting for transfers between devices, per_device(): lax.all_gather(values, 'sp', axis=0, tiled=True)  29 us
    all_gather x1, waiting for transfers between devices, per_device(): lax.all_gather(tokens, 'tp', axis=1, tiled=True)  26.6 us
    dot_general x4, matrix products, block_scores(): jnp.einsum('qhcd,khcd->hcqk', queries, key_block, preferred_element_type=...  20.8 us
    all_gather x1, waiting for transfers between devices, per_device(): lax.all_gather(conv_out, 'tp', axis=1, tiled=True)  16.8 us
    dot_general x6, matrix products, add_products(): jnp.dot(scaled, weight, preferred_element_type=jnp.float32)  10.6 us
    reduce_sum x2, other arithmetic, stats_step(): jnp.sum(exponent, axis=-1)  8.38 us
    all_gather x1, waiting for transfers between devices, per_device(): lax.all_gather(attn_out, 'tp', axis=1, tiled=True)  5.45 us
  transfers between devices with their start and end apart: 6, of which 6 were waited for; matrix products, arithmetic and copies ran while one was open for 15% of the time, Pallas kernels for 0%

commit v1 on v0

v1 whole, which is shorter than its diff:
```python
import functools
import math

import jax
import jax.numpy as jnp
from jax import lax
from jax.experimental import pallas as pl
from jax.experimental.pallas import tpu as pltpu
from jax.sharding import PartitionSpec as P

NORM_EPS = 1e-06
HEAD_EPS = 1e-05
ROPE_BASE = 500000.0
MASKED = -1e30
HEAD_SCALE = 0.8
VMEM_BYTES = 56 * 1024 * 1024


def shifted(block, axis, distance):
    devices = range(lax.axis_size(axis))
    route = [(i - distance, i) for i in devices if i - distance in devices]
    return lax.ppermute(block, axis, route)


def turn_tables(positions, head_dim, columns):
    half_dim = head_dim // 2
    frequency = ROPE_BASE ** (-jnp.arange(half_dim, dtype=jnp.float32) * 2.0 / head_dim)
    angles = positions[:, None] * jnp.tile(frequency, columns // half_dim)[None, :]
    sign = jnp.where((jnp.arange(columns) % head_dim) < half_dim, -1.0, 1.0)
    return jnp.cos(angles), jnp.sin(angles) * sign[None, :]


def project_kernel(
    tok_ref, gain_ref, cos_ref, sin_ref, wq, wk, wv, wo, wi, ws,
    q_ref, kv_ref, cin_ref, gate_ref, *, head_dim,
):
    floats = tok_ref[...].astype(jnp.float32)
    squares = jnp.sum(floats * floats, axis=1, keepdims=True)
    inverse_rms = lax.rsqrt(squares / floats.shape[1] + NORM_EPS)
    scaled = (floats * gain_ref[...]).astype(jnp.bfloat16)
    columns = wq.shape[1]
    lanes = cos_ref.shape[1]
    half = head_dim // 2

    def project(w):
        return jnp.dot(scaled, w[...], preferred_element_type=jnp.float32) * inverse_rms

    low = lax.broadcasted_iota(jnp.int32, (floats.shape[0], lanes), 1) % head_dim < half
    cosine = cos_ref[...]
    sine = sin_ref[...]

    def turned(raw):
        parts = []
        for start in range(0, columns, lanes):
            part = raw[:, start : start + lanes]
            other = jnp.where(
                low, pltpu.roll(part, lanes - half, 1), pltpu.roll(part, half, 1)
            )
            parts.append((part * cosine + other * sine).astype(jnp.bfloat16))
        return parts

    for index, part in enumerate(turned(project(wk))):
        kv_ref[:, index * lanes : (index + 1) * lanes] = part
    kv_ref[:, columns:] = project(wv).astype(jnp.bfloat16)
    for index, part in enumerate(turned(project(wq))):
        q_ref[:, index * lanes : (index + 1) * lanes] = part
    inner = project(wi).astype(jnp.bfloat16).astype(jnp.float32)
    signal = project(ws).astype(jnp.bfloat16).astype(jnp.float32)
    cin_ref[...] = (inner * signal).astype(jnp.bfloat16)
    gate_ref[...] = project(wo).astype(jnp.bfloat16)


def project_all(tokens, gain, cosine, sine, weights, head_dim):
    rows, width = tokens.shape
    columns = weights[0].shape[1]
    lanes = cosine.shape[1]
    tile = math.gcd(rows, 256)
    row_block = lambda n: pl.BlockSpec((tile, n), lambda i: (i, 0))
    whole = pl.BlockSpec((width, columns), lambda i: (0, 0))
    shape = lambda n: jax.ShapeDtypeStruct((rows, n), jnp.bfloat16)
    return pl.pallas_call(
        functools.partial(project_kernel, head_dim=head_dim),
        grid=(rows // tile,),
        in_specs=[row_block(width), pl.BlockSpec((1, width), lambda i: (0, 0)),
                  row_block(lanes), row_block(lanes)] + [whole] * 6,
        out_specs=[row_block(columns), row_block(2 * columns), row_block(columns), row_block(columns)],
        out_shape=[shape(columns), shape(2 * columns), shape(columns), shape(columns)],
        compiler_params=pltpu.CompilerParams(
            dimension_semantics=("arbitrary",), vmem_limit_bytes=VMEM_BYTES),
        cost_estimate=pl.CostEstimate(
            flops=12 * rows * width * columns, transcendentals=rows,
            bytes_accessed=2 * (rows * width + 6 * width * columns + 5 * rows * columns)),
        name="project",
    )(tokens, gain, cosine, sine, *weights)


def attend_kernel(
    place_ref, lambda_ref, q_ref, k_ref, v_ref, gain_ref, out_ref, totals_ref, s_ref,
    *, local_rows, block, head_dim,
):
    tile = q_ref.shape[0]
    value_dim = v_ref.shape[1]
    head = pl.program_id(0)
    row_start = place_ref[0] * local_rows + pl.program_id(1) * tile
    full_blocks = row_start // block
    queries = q_ref[...] * jnp.asarray(head_dim ** (-0.5), jnp.bfloat16)
    first = lax.broadcasted_iota(jnp.int32, queries.shape, 1) < head_dim
    zero = jnp.zeros_like(queries)
    stacked = jnp.concatenate(
        [jnp.where(first, queries, zero), jnp.where(first, zero, queries)], axis=0
    )
    groups = range(0, block, 128)

    def scores_of(index):
        keys = k_ref[pl.ds(index * block, block), :]
        return lax.dot_general(
            stacked, keys, (((1,), (1,)), ((), ())), preferred_element_type=jnp.float32
        )

    def lane_max(running, scores):
        for g in groups:
            running = jnp.maximum(running, scores[:, g : g + 128])
        return running

    def score_step(index, running):
        scores = scores_of(index)
        s_ref[:, pl.ds(index * block, block)] = scores
        return lane_max(running, scores)

    running = lax.fori_loop(
        0, full_blocks, score_step, jnp.full((2 * tile, 128), MASKED, jnp.float32)
    )
    scores = scores_of(full_blocks)
    row_ids = lax.broadcasted_iota(jnp.int32, scores.shape, 0) % tile + row_start
    col_ids = lax.broadcasted_iota(jnp.int32, scores.shape, 1) + full_blocks * block
    scores = jnp.where(row_ids >= col_ids, scores, MASKED)
    s_ref[:, pl.ds(full_blocks * block, block)] = scores
    row_max = jnp.max(lane_max(running, scores), axis=1, keepdims=True)

    def exp_step(index, running):
        exponent = jnp.exp(s_ref[:, pl.ds(index * block, block)] - row_max)
        s_ref[:, pl.ds(index * block, block)] = exponent
        for g in groups:
            running = running + exponent[:, g : g + 128]
        return running

    running = lax.fori_loop(
        0, full_blocks + 1, exp_step, jnp.zeros((2 * tile, 128), jnp.float32)
    )
    row_sum = jnp.sum(running, axis=1, keepdims=True)
    totals_ref[0] = row_max + jnp.log(row_sum)
    factor = 1.0 / row_sum
    plus = factor[:tile]
    minus = factor[tile:] * lambda_ref[head]

    def value_step(index, running):
        window = pl.ds(index * block, block)
        weights = s_ref[:tile, window] * plus - s_ref[tile:, window] * minus
        return running + jnp.dot(
            weights.astype(jnp.bfloat16), v_ref[window, :], preferred_element_type=jnp.float32
        )

    head_mix = lax.fori_loop(
        0, full_blocks + 1, value_step, jnp.zeros((tile, value_dim), jnp.float32)
    )
    mean_square = jnp.mean(head_mix * head_mix, axis=1, keepdims=True)
    normed = head_mix * lax.rsqrt(mean_square + HEAD_EPS) * gain_ref[...] * HEAD_SCALE
    out_ref[...] = normed.astype(jnp.bfloat16)


def attend(place, lambdas, queries, keys_values, head_gain, head_dim):
    local_rows, columns = queries.shape
    tokens_all = keys_values.shape[0]
    heads = lambdas.shape[0]
    value_dim = 2 * head_dim
    tile = math.gcd(local_rows, 256)
    if tokens_all * tile * 8 > 16 * 1024 * 1024:
        tile = math.gcd(local_rows, 128)
    block = math.gcd(local_rows, 512)
    block = max(block, tile)
    tiles = local_rows // tile
    smem = pl.BlockSpec(memory_space=pltpu.SMEM)
    out, totals = pl.pallas_call(
        functools.partial(attend_kernel, local_rows=local_rows, block=block, head_dim=head_dim),
        grid=(heads, tiles),
        in_specs=[
            smem, smem,
            pl.BlockSpec((tile, value_dim), lambda h, i: (i, h)),
            pl.BlockSpec((tokens_all, value_dim), lambda h, i: (0, h)),
            pl.BlockSpec((tokens_all, value_dim), lambda h, i: (0, heads + h)),
            pl.BlockSpec((1, value_dim), lambda h, i: (0, 0)),
        ],
        out_specs=[
            pl.BlockSpec((tile, value_dim), lambda h, i: (i, h)),
            pl.BlockSpec((1, 2 * tile, 1), lambda h, i: (h * tiles + i, 0, 0)),
        ],
        out_shape=[
            jax.ShapeDtypeStruct((local_rows, columns), jnp.bfloat16),
            jax.ShapeDtypeStruct((heads * tiles, 2 * tile, 1), jnp.float32),
        ],
        scratch_shapes=[pltpu.VMEM((2 * tile, tokens_all), jnp.float32)],
        compiler_params=pltpu.CompilerParams(
            dimension_semantics=("arbitrary", "arbitrary"), vmem_limit_bytes=VMEM_BYTES),
        cost_estimate=pl.CostEstimate(
            flops=8 * heads * local_rows * tokens_all * value_dim,
            transcendentals=2 * heads * local_rows * tokens_all,
            bytes_accessed=4 * tokens_all * columns),
        name="attend",
    )(place, lambdas, queries, keys_values, keys_values, head_gain)
    totals = totals.reshape(heads, tiles, 2, tile).transpose(0, 2, 1, 3)
    return out, totals.reshape(heads, 2, local_rows)


def per_device(
    tokens,
    norm_gain,
    query_weight,
    key_weight,
    value_weight,
    outer_gate_weight,
    inner_gate_weight,
    conv_input_weight,
    conv_taps,
    lambdas,
    head_gain,
    attn_out_weight,
    conv_out_weight,
):
    local_rows = tokens.shape[0]
    local_heads = lambdas.shape[0]
    head_dim = query_weight.shape[1] // (2 * local_heads)
    taps_count = conv_taps.shape[0]
    columns_dev = query_weight.shape[1]
    place = lax.axis_index("sp").astype(jnp.int32)
    positions = (
        place * local_rows + jnp.arange(local_rows, dtype=jnp.int32)
    ).astype(jnp.float32)
    cosine, sine = turn_tables(positions, head_dim, 2 * head_dim)
    queries, keys_values, conv_in, outer_gate = project_all(
        lax.all_gather(tokens, "tp", axis=1, tiled=True),
        norm_gain[None, :], cosine, sine,
        (query_weight, key_weight, value_weight, outer_gate_weight,
         inner_gate_weight, conv_input_weight),
        head_dim,
    )
    all_keys_values = lax.all_gather(keys_values, "sp", axis=0, tiled=True)
    rim_rows = shifted(conv_in[local_rows - (taps_count - 1) :], "sp", 1)
    padded = jnp.concatenate([rim_rows, conv_in], axis=0)
    summed = jnp.zeros((local_rows, columns_dev), jnp.float32)
    for tap_index in range(taps_count):
        summed = summed + conv_taps[tap_index][None, :] * padded[
            tap_index : tap_index + local_rows
        ].astype(jnp.float32)
    conv_out = (outer_gate.astype(jnp.float32) * summed).astype(jnp.bfloat16)
    conv_all = lax.all_gather(conv_out, "tp", axis=1, tiled=True)
    attn_out, log_totals = attend(
        place[None], lambdas, queries, all_keys_values, head_gain[None, :], head_dim
    )
    conv_part = jnp.dot(conv_all, conv_out_weight, preferred_element_type=jnp.float32)
    mixed_out = conv_part + jnp.dot(
        lax.all_gather(attn_out, "tp", axis=1, tiled=True),
        attn_out_weight,
        preferred_element_type=jnp.float32,
    )
    return (mixed_out.astype(jnp.bfloat16), log_totals)


def solution(mesh):
    in_specs = (
        P("sp", "tp"),
        P(),
        P(None, "tp"),
        P(None, "tp"),
        P(None, "tp"),
        P(None, "tp"),
        P(None, "tp"),
        P(None, "tp"),
        P(None, "tp"),
        P("tp"),
        P(),
        P(None, "tp"),
        P(None, "tp"),
    )
    out_specs = (P("sp", "tp"), P("tp", None, "sp"))
    return jax.shard_map(
        per_device, mesh=mesh, in_specs=in_specs, out_specs=out_specs, check_vma=False
    )
```

time: 212 us -> 167 us (0.79)
  matrix products: 38.8 us -> 5.98 us
  Pallas kernels: 0 us -> 14.9 us
  other arithmetic: 19.3 us -> 4.4 us
  local copies, waits for them, and re-layouts: 7.83 us -> 1.43 us
  waiting for transfers between devices: 126 us -> 123 us
  loops' own time: 2.83 us -> 0 us
    dot_general x13 -> x1, matrix products: 36.8 us -> 2.94 us  [per_device(): jnp.dot(conv_all, conv_out_weight, preferred_element_type=jnp.float32)]
    all_gather x3 -> x2, waiting for transfers between devices: 91 us -> 75 us  [the longest x1 65.3 us: per_device(): all_keys_values = lax.all_gather(keys_values, 'sp', axis=0, tiled=True)]
    all_gather x1, waiting for transfers between devices: 5.45 us -> 21 us  [per_device(): lax.all_gather(attn_out, 'tp', axis=1, tiled=True)]
    pallas_call x0 -> x2, Pallas kernels: none -> 14.9 us  [the longest x1 7.65 us: project_all(): pl.pallas_call(functools.partial(project_kernel, head_dim=head_dim), grid...]
    reduce_sum x4 -> x0, other arithmetic: 11.7 us -> none  [the longest x2 8.38 us: stats_step(): jnp.sum(exponent, axis=-1)]
    ge x4 -> x0, other arithmetic: 3.05 us -> none  [block_scores(): query_pos[:, None]]
    reshape x2 -> x1, local copies, waits for them, and re-layouts: 3.52 us -> 0.63 us  [attend(): totals = totals.reshape(heads, tiles, 2, tile).transpose(0, 2, 1, 3)]
    another operation x2 -> x0, loops' own time: 2.83 us -> none  [over_shards(): lax.scan(scan_step, running, (stacked, jnp.arange(steps_count, dtype=jnp....]
  transfers between devices with their start and end apart: 6 -> 5, of which waited for: 6 -> 5; matrix products, arithmetic and copies ran while one was open for 15% -> 5% of each run, Pallas kernels for 0% -> 4%
where the time goes in v1:
time: 167 us
  waiting for transfers between devices  123 us (74%)
  Pallas kernels  14.9 us (9%)
  between operations  13.8 us (8%)
  matrix products  5.98 us (4%)
  other arithmetic  4.4 us (3%)
  starting transfers between devices  3.53 us (2%)
    all_gather x1, waiting for transfers between devices, per_device(): all_keys_values = lax.all_gather(keys_values, 'sp', axis=0, tiled=True)  65.3 us
    all_gather x1, waiting for transfers between devices, per_device(): lax.all_gather(tokens, 'tp', axis=1, tiled=True)  25 us
    all_gather x1, waiting for transfers between devices, per_device(): lax.all_gather(attn_out, 'tp', axis=1, tiled=True)  21 us
    all_gather x1, waiting for transfers between devices, per_device(): conv_all = lax.all_gather(conv_out, 'tp', axis=1, tiled=True)  9.71 us
    pallas_call x1, Pallas kernels, project_all(): pl.pallas_call(functools.partial(project_kernel, head_dim=head_dim), grid...  7.65 us
    pallas_call x1, Pallas kernels, attend(): pl.pallas_call(functools.partial(attend_kernel, local_rows=local_rows, bl...  7.2 us
    ppermute x1, starting transfers between devices, shifted(): return lax.ppermute(block, axis, route)  3.37 us
  transfers between devices with their start and end apart: 5, of which 5 were waited for; matrix products, arithmetic and copies ran while one was open for 5% of the time, Pallas kernels for 4%

profile of v1, /device:TPU:0, one launch (start us, length us, event | category | flops | bytes accessed | tf_op | source)
XLA Modules:
  0.0 166.9 jit_solution(7959371942412053906)
XLA Ops:
  7.2 0.0 all-gather.5.cloned.1.call-start
  7.2 0.7 all-gather.5.cloned.1.call-update
  7.9 0.0 all-gather.9.cloned.1.call-start
  8.0 0.1 mul.64
  8.1 1.8 %fusion.2 = (f32[512,128]{1,0:T(8,128)}, f32[512,128]{1,0:T(8,128)}) fusion(f32[128]{0:T(128)S(1)} %compare_select_fusion, f32[128]{0:T(128)S(1)} %mul.64, f32[512]{0:T(512)S(1)} %add_convert_fusion), kind=kLoop, calls=%fused_computation.8 | loop fusion | flops 131072 | bytes 527360 | tf_op jit(solution)/shard_map/mul | solution.py:30
  9.9 25.0 %all-gather.5.cloned.1.call-done.tok_ref = bf16[512,2048]{1,0:T(8,128)(2,1)} async-done(((bf16[512,512]{1,0:T(8,128)(2,1)}), bf16[512,2048]{1,0:T(8,128)(2,1)}) %all-gather.5.cloned.1.call-update) | async-done | bytes 2097168 | tf_op jit(solution)/shard_map/all_gather | solution.py:240
  34.9 7.7 %project.1 = (bf16[512,256]{1,0:T(8,128)(2,1)}, bf16[512,512]{1,0:T(8,128)(2,1)}, bf16[512,256]{1,0:T(8,128)(2,1)}, bf16[512,256]{1,0:T(8,128)(2,1)}) custom-call(bf16[512,2048]{1,0:T(8,128)(2,1)} %all-gather.5.cloned.1.call-done.tok_ref, f32[1,2048]{1,0:T(1,128)} %bitcast.17, f32[512,128]{1,0:T(8,128)} %get-tuple-element.18.cos_ref, ...), custom_call_target="tpu_custom_call" | custom-call | flops 3221225472 | bytes 9699328 | tf_op jit(solution)/shard_map/project/pallas_call | solution.py:81
  42.5 0.0 all-gather.9.cloned.1.call-update
  42.5 0.0 all-gather.7.cloned.1.call-start
  42.6 0.7 slice.19
  43.3 3.4 %collective-permute-start = (bf16[2,256]{1,0:T(2,128)(2,1)S(1)}, bf16[2,256]{1,0:T(2,128)(2,1)S(1)}, u32[]{:S(2)}, u32[]{:S(2)}) collective-permute-start(bf16[2,256]{1,0:T(2,128)(2,1)S(1)} %slice.19), channel_id=1, source_target_pairs={{0,4},{4,8},{8,12},{12,16},{16,20},{20,24},{24,28},{1,5},{5,9},{9,... | collective-permute-start | bytes 3080 | tf_op jit(solution)/shard_map/ppermute | solution.py:22
  46.7 1.3 collective-permute-done
  47.9 2.2 %multiply_convert_fusion = bf16[512,256]{1,0:T(8,128)(2,1)} fusion(bf16[512,256]{1,0:T(8,128)(2,1)} %get-tuple-element.9, bf16[512,256]{1,0:T(8,128)(2,1)} %get-tuple-element.8, bf16[2,256]{1,0:T(2,128)(2,1)S(1)} %collective-permute-done, f32[256]{0:T(256)S(1)} %bitcast.15, f32[256]{0:T(256)S(1)} %bitcast.16, f32[256]{0:T(256)S(1)} %bitcast.14), kind=kLoop, calls=%fused_computation.2 | loop fusion | flops 2228224 | bytes 790528 | tf_op jit(solution)/shard_map/convert_element_type | solution.py:254
  50.2 0.0 all-gather.7.cloned.1.call-update
  50.2 0.0 all-gather.11.cloned.1.call-start
  50.2 65.3 %all-gather.9.cloned.1.call-done.k_ref.v_ref = bf16[4096,512]{1,0:T(8,128)(2,1)} async-done(((bf16[512,512]{1,0:T(8,128)(2,1)}), bf16[4096,512]{1,0:T(8,128)(2,1)}) %all-gather.9.cloned.1.call-update) | async-done | bytes 4194320 | tf_op jit(solution)/shard_map/all_gather | solution.py:246
  115.5 7.2 %attend.1 = (bf16[512,256]{1,0:T(8,128)(2,1)}, f32[4,512,1]{2,1,0:T(8,128)}) custom-call(s32[1]{0:T(128)} %bitcast.4.place_ref, f32[2]{0:T(128)} %lambda_ref.1, bf16[512,256]{1,0:T(8,128)(2,1)} %get-tuple-element.10.q_ref, bf16[4096,512]{1,0:T(8,128)(2,1)} %all-gather.9.cloned.1.call-done.k_ref.v_ref, ...), custom_call_target="tpu_custom_call" | custom-call | flops 4294967296 | bytes 4194304 | tf_op jit(solution)/shard_map/attend/pallas_call | solution.py:183
  122.7 0.0 all-gather.11.cloned.1.call-update
  122.7 9.7 %all-gather.7.cloned.1.call-done = bf16[512,1024]{1,0:T(8,128)(2,1)} async-done(((bf16[512,256]{1,0:T(8,128)(2,1)}), bf16[512,1024]{1,0:T(8,128)(2,1)}) %all-gather.7.cloned.1.call-update) | async-done | bytes 1048592 | tf_op jit(solution)/shard_map/all_gather | solution.py:255
  132.4 2.9 %fusion.4 = f32[512,512]{1,0:T(8,128)} fusion(bf16[512,1024]{1,0:T(8,128)(2,1)} %all-gather.7.cloned.1.call-done, bf16[1024,512]{1,0:T(8,128)(2,1)S(1)} %copy-done), kind=kOutput, calls=%fused_computation.15 | convolution fusion | flops 536870912 | bytes 3145728 | tf_op jit(solution)/shard_map/dot_general | solution.py:259
  135.4 0.3 reduce
  135.7 0.6 reshape.33
  136.4 21.0 %all-gather.11.cloned.1.call-done = bf16[512,1024]{1,0:T(8,128)(2,1)} async-done(((bf16[512,256]{1,0:T(8,128)(2,1)}), bf16[512,1024]{1,0:T(8,128)(2,1)}) %all-gather.11.cloned.1.call-update) | async-done | bytes 1048592 | tf_op jit(solution)/shard_map/all_gather | solution.py:261
  157.4 3.0 %fusion = bf16[512,512]{1,0:T(8,128)(2,1)} fusion(f32[512,512]{1,0:T(8,128)} %fusion.4, bf16[512,1024]{1,0:T(8,128)(2,1)} %all-gather.11.cloned.1.call-done, bf16[1024,512]{1,0:T(8,128)(2,1)S(1)} %copy-done.3), kind=kOutput, calls=%fused_computation.1 | convolution fusion | flops 537395200 | bytes 3670016 | tf_op jit(solution)/shard_map/dot_general | solution.py:260
  (13 shorter events, 0.0 us)
Async XLA Ops:
  7.2 125.3 %copy-start = (bf16[1024,512]{1,0:T(8,128)(2,1)S(1)}, bf16[1024,512]{1,0:T(8,128)(2,1)}, u32[]{:S(2)}) copy-start(bf16[1024,512]{1,0:T(8,128)(2,1)} %param.25) | copy-start | bytes 3145732
  7.2 27.7 %all-gather.5.cloned.1.call-start = ((), (), s32[]{:S(2)}) async-start(), calls=%async_computation | async-start | bytes 2621440 | tf_op jit(solution)/shard_map/all_gather | solution.py:240
  7.9 107.6 %all-gather.9.cloned.1.call-start = ((), (), s32[]{:S(2)}) async-start(), calls=%async_computation.2 | async-start | bytes 4718592 | tf_op jit(solution)/shard_map/all_gather | solution.py:246
  34.9 11.8 %copy-start.2 = (f32[3,256]{1,0:T(4,128)S(1)}, f32[3,256]{1,0:T(4,128)}, u32[]{:S(2)}) copy-start(f32[3,256]{1,0:T(4,128)} %param.21) | copy-start | bytes 9220
  42.5 89.9 %all-gather.7.cloned.1.call-start = ((), (), s32[]{:S(2)}) async-start(), calls=%async_computation.1 | async-start | bytes 1310720 | tf_op jit(solution)/shard_map/all_gather | solution.py:255
  43.3 4.7 %collective-permute-start = (bf16[2,256]{1,0:T(2,128)(2,1)S(1)}, bf16[2,256]{1,0:T(2,128)(2,1)S(1)}, u32[]{:S(2)}, u32[]{:S(2)}) collective-permute-start(bf16[2,256]{1,0:T(2,128)(2,1)S(1)} %slice.19), channel_id=1, source_target_pairs={{0,4},{4,8},{8,12},{12,16},{16,20},{20,24},{24,28},{1,5},{5,9},{9,... | collective-permute-start | bytes 3080 | tf_op jit(solution)/shard_map/ppermute | solution.py:22
  50.2 107.2 %all-gather.11.cloned.1.call-start = ((), (), s32[]{:S(2)}) async-start(), calls=%async_computation.3 | async-start | bytes 1310720 | tf_op jit(solution)/shard_map/all_gather | solution.py:261
  122.7 12.7 %copy-start.1 = (f32[4,512,1]{2,1,0:T(8,128)S(1)}, f32[4,512,1]{2,1,0:T(8,128)}, u32[]{:S(2)}) copy-start(f32[4,512,1]{2,1,0:T(8,128)} %get-tuple-element.13) | copy-start | bytes 24580
  122.7 34.7 %copy-start.3 = (bf16[1024,512]{1,0:T(8,128)(2,1)S(1)}, bf16[1024,512]{1,0:T(8,128)(2,1)}, u32[]{:S(2)}) copy-start(bf16[1024,512]{1,0:T(8,128)(2,1)} %param.24) | copy-start | bytes 3145732
Sparse Core Ops, SparseCore 0:
  9.5 25.2 all-gather.4
  42.7 72.7 all-gather.8
  117.1 15.3 all-gather.6
  134.4 22.8 all-gather.10
